TPU v7x, 32 devices: a whole 2x2x4 slice. The times are simulated.
32 devices in a mesh: ep: 8 (over z, x), tp: 4 (over y, core).
Axes of the slice: x: 2, y: 2, z: 4, core: 2. Of those that a mesh axis runs over, the one named last changes fastest.
Arguments:
- tokens: bfloat16 [512, 4096], P('ep'), may hold values from -6 to 6
- state_in: float32 [512, 4096], P('ep', 'tp'), may hold values from -6 to 6
- conv_in: bfloat16 [512, 3, 4096], P('ep', None, 'tp'), may hold values from -6 to 6
- mix_gain: bfloat16 [4096], replicated, may hold values from 0.099609375 to 1.8984375
- rnn_weight: bfloat16 [4096, 4096], P('ep', 'tp'), may hold values from -0.09375 to 0.09375
- gate_weight: bfloat16 [4096, 4096], P('ep', 'tp'), may hold values from -0.09375 to 0.09375
- conv_weight: bfloat16 [4, 4096], P(None, 'tp'), may hold values from -3 to 3
- rate_weight: bfloat16 [16, 256, 256], P('tp'), may hold values from -0.375 to 0.375
- input_weight: bfloat16 [16, 256, 256], P('tp'), may hold values from -0.375 to 0.375
- rate_param: float32 [4096], P('tp'), may hold values from 1 to 6
- out_weight: bfloat16 [4096, 4096], P('tp'), may hold values from -0.09375 to 0.09375
- moe_gain: bfloat16 [4096], replicated, may hold values from 0.099609375 to 1.8984375
- expert_gate: bfloat16 [8, 4096, 2048], P('ep', None, 'tp'), may hold values from -0.09375 to 0.09375
- expert_up: bfloat16 [8, 4096, 2048], P('ep', None, 'tp'), may hold values from -0.09375 to 0.09375
- expert_down: bfloat16 [8, 2048, 4096], P('ep', 'tp'), may hold values from -0.125 to 0.125
- routes: int32 [512, 2], P('ep'), may hold values from 0 to 7, all different within a row; in each aligned block of 64 rows (0 to 63, 64 to 127, ...) at most 32 rows name the same one
- route_prob: float32 [512, 2], P('ep'), may hold values from 0.1 to 1
Outputs:
- layer_out: bfloat16 [512, 4096], P('ep', 'tp')
- state_out: float32 [512, 4096], P('ep', 'tp')
- conv_out: bfloat16 [512, 3, 4096], P('ep', None, 'tp')
Inputs may be any that keep to these rules, and one draw needn't show every extreme that they name: `routes`: the 2 experts of a sequence differ. Among the rows of one index of ep no expert is named more than 32 times, and in every draw some expert is named exactly 32 times there.
All inputs are finite; a program needn't handle non-finite values.
Results may differ from a plain program's by a relative error of at most 0.014.
Values may be sent and summed in bfloat16 or wider, within the bound.
A program may use at most 64 MiB of HBM per device.

v0:
```python
import jax
import jax.numpy as jnp
from jax import lax
from jax.sharding import PartitionSpec as P


def rms_scale(values, gain):
    scale = lax.rsqrt(jnp.mean(values * values, axis=-1, keepdims=True) + 1e-06)
    return values * scale * gain.astype(jnp.float32)


def slot_targets(route_ids, experts, capacity):
    flat_ids = route_ids.reshape(-1)
    onehot = (flat_ids[:, None] == jnp.arange(experts, dtype=jnp.int32)[None, :]).astype(jnp.int32)
    before = jnp.cumsum(onehot, axis=0) - onehot
    slot_ids = jnp.sum(before * onehot, axis=1)
    return flat_ids * capacity + slot_ids


def block_map(conv, weight):
    rows = conv.shape[0]
    blocks = weight.shape[0]
    parts = conv.reshape(rows, blocks, weight.shape[1])
    mapped = jnp.einsum("snc,ncd->snd", parts, weight, preferred_element_type=jnp.float32)
    return mapped.reshape(rows, blocks * weight.shape[2])


def shards(
    tokens,
    state_in,
    conv_in,
    mix_gain,
    rnn_weight,
    gate_weight,
    conv_weight,
    rate_weight,
    input_weight,
    rate_param,
    out_weight,
    moe_gain,
    expert_gate,
    expert_up,
    expert_down,
    routes,
    route_prob,
):
    group_rows = tokens.shape[0]
    model_width = tokens.shape[1]
    channels = rnn_weight.shape[1]
    base = tokens.astype(jnp.float32)
    normed = rms_scale(base, mix_gain).astype(jnp.bfloat16)
    columns = lax.all_to_all(normed, "ep", split_axis=1, concat_axis=0, tiled=True)
    joined = jnp.concatenate([rnn_weight, gate_weight], axis=1)
    summed = lax.psum_scatter(
        jnp.dot(columns, joined, preferred_element_type=jnp.float32).astype(jnp.bfloat16),
        "ep",
        scatter_dimension=0,
        tiled=True,
    ).astype(jnp.float32)
    proj_x = summed[:, :channels]
    proj_y = summed[:, channels:]
    moved = proj_x.astype(jnp.bfloat16)
    conv_out = jnp.concatenate([conv_in[:, 1:], moved[:, None, :]], axis=1)
    taps = conv_weight.astype(jnp.float32)
    history = conv_in.astype(jnp.float32)
    mixed_in = (
        history[:, 0] * taps[0]
        + history[:, 1] * taps[1]
        + history[:, 2] * taps[2]
        + moved.astype(jnp.float32) * taps[3]
    )
    conv = mixed_in.astype(jnp.bfloat16)
    rate = jax.nn.sigmoid(block_map(conv, rate_weight))
    in_gate = jax.nn.sigmoid(block_map(conv, input_weight))
    log_decay = -8.0 * rate * jax.nn.softplus(-rate_param)
    state_out = jnp.exp(log_decay) * state_in + jnp.sqrt(
        -jnp.expm1(2.0 * log_decay)
    ) * in_gate * conv.astype(jnp.float32)
    gated = (state_out * jax.nn.gelu(proj_y, approximate=True)).astype(jnp.bfloat16)
    partial_out = jnp.dot(gated, out_weight, preferred_element_type=jnp.float32)
    mixed = base + lax.psum(partial_out.astype(jnp.bfloat16), "tp").astype(jnp.float32)
    normed2 = rms_scale(mixed, moe_gain).astype(jnp.bfloat16)
    experts = lax.axis_size("ep")
    topk = routes.shape[1]
    capacity = max(2, 2 * group_rows * topk // experts)
    targets = slot_targets(routes, experts, capacity)
    dispatch = (
        jnp.arange(experts * capacity, dtype=jnp.int32)[:, None] == targets[None, :]
    ).astype(jnp.bfloat16)
    repeated = jnp.repeat(normed2, topk, axis=0)
    send = jnp.dot(dispatch, repeated, preferred_element_type=jnp.float32).astype(jnp.bfloat16)
    send = send.reshape(experts, capacity, model_width)
    received = lax.all_to_all(send, "ep", split_axis=0, concat_axis=0, tiled=True)
    flat_rows = received.reshape(-1, model_width)
    gate_part = jnp.dot(flat_rows, expert_gate[0], preferred_element_type=jnp.float32)
    up_part = jnp.dot(flat_rows, expert_up[0], preferred_element_type=jnp.float32)
    hidden = (jax.nn.silu(gate_part) * up_part).astype(jnp.bfloat16)
    result = jnp.dot(hidden, expert_down[0], preferred_element_type=jnp.float32)
    partial_experts = result.reshape(received.shape[0], received.shape[1], model_width)
    reduced = lax.psum_scatter(
        partial_experts.astype(jnp.bfloat16), "tp", scatter_dimension=2, tiled=True
    )
    returned = lax.all_to_all(reduced, "ep", split_axis=0, concat_axis=0, tiled=True)
    share = returned.shape[2]
    picked = jnp.einsum(
        "rj,rd->jd",
        dispatch,
        returned.reshape(experts * capacity, share),
        preferred_element_type=jnp.float32,
    )
    weights = route_prob / jnp.sum(route_prob, axis=1, keepdims=True)
    experts_sum = jnp.sum(picked.reshape(group_rows, topk, share) * weights[:, :, None], axis=1)
    own_columns = lax.dynamic_slice_in_dim(mixed, lax.axis_index("tp") * share, share, 1)
    layer_out = (own_columns + experts_sum).astype(jnp.bfloat16)
    return (layer_out, state_out, conv_out)


def solution(mesh):
    in_specs = (
        P("ep", None),
        P("ep", "tp"),
        P("ep", None, "tp"),
        P(),
        P("ep", "tp"),
        P("ep", "tp"),
        P(None, "tp"),
        P("tp", None, None),
        P("tp", None, None),
        P("tp"),
        P("tp", None),
        P(),
        P("ep", None, "tp"),
        P("ep", None, "tp"),
        P("ep", "tp", None),
        P("ep", None),
        P("ep", None),
    )
    out_specs = (P("ep", "tp"), P("ep", "tp"), P("ep", None, "tp"))
    return jax.shard_map(shards, mesh=mesh, in_specs=in_specs, out_specs=out_specs, check_vma=False)
```

profile of v0, /device:TPU:0, one launch (start us, length us, event | category | flops | bytes accessed | tf_op | source)
XLA Modules:
  0.0 267.9 jit_solution(9502218566155616131)
XLA Ops:
  7.2 0.7 convert_element_type.63
  8.0 1.2 fusion.23
  9.2 1.2 fusion.25
  10.5 21.6 %all_to_all.29 = bf16[64,8,512]{2,0,1:T(8,128)(2,1)S(1)} all-to-all(bf16[64,8,512]{2,0,1:T(8,128)(2,1)S(1)} %bitcast.85), channel_id=1, replica_groups=mesh['ep'=8,'tp'=4] {'ep'}, dimensions={1} | all-to-all | bytes 1048576 | tf_op jit(solution)/shard_map/all_to_all | solution.py:52
  32.1 4.2 %convolution_convert_fusion.3 = bf16[512,2048]{1,0:T(8,128)(2,1)} fusion(bf16[512,512]{1,0:T(8,128)(2,1)S(1)} %bitcast.88, bf16[512,1024]{1,0:T(8,128)(2,1)} %param.22, bf16[512,1024]{1,0:T(8,128)(2,1)} %param.21), kind=kOutput, calls=%fused_computation.8 | convolution fusion | flops 1078984704 | bytes 4718592 | tf_op jit(solution)/shard_map/dot_general | solution.py:55
  37.1 66.8 %reduce-scatter.3.cloned.1.call-done = bf16[64,2048]{1,0:T(8,128)(2,1)} async-done(((bf16[512,2048]{1,0:T(8,128)(2,1)}), bf16[64,2048]{1,0:T(8,128)(2,1)}) %reduce-scatter.3.cloned.1.call-update) | async-done | bytes 262160 | tf_op jit(solution)/shard_map/reduce_scatter | solution.py:54
  103.8 1.1 fusion.36
  105.8 5.9 %convolution_convert_fusion.2 = bf16[64,4096]{1,0:T(8,128)(2,1)} fusion(bf16[1024,4096]{1,0:T(8,128)(2,1)} %param.27, f32[64,1024]{1,0:T(8,128)S(1)} %multiply_add_fusion, bf16[64,2048]{1,0:T(8,128)(2,1)S(1)} %copy-done.4), kind=kOutput, calls=%fused_computation.2 | convolution fusion | flops 537853952 | bytes 9306112 | tf_op jit(solution)/shard_map/dot_general | solution.py:80
  111.9 32.4 %all-reduce.2.cloned.1.call-done = bf16[64,4096]{1,0:T(8,128)(2,1)} async-done(((bf16[64,4096]{1,0:T(8,128)(2,1)}), bf16[64,4096]{1,0:T(8,128)(2,1)}) %all-reduce.2.cloned.1.call-update) | async-done | bytes 524304 | tf_op jit(solution)/shard_map/psum | solution.py:81
  144.3 2.3 convert_add_fusion
  146.6 1.3 multiply_convert_fusion
  147.9 1.0 broadcast_in_dim.4
  149.4 0.7 convolution_convert_fusion
  150.1 52.8 %all_to_all.30 = bf16[8,32,4096]{2,1,0:T(8,128)(2,1)S(1)} all-to-all(bf16[8,32,4096]{2,1,0:T(8,128)(2,1)S(1)} %bitcast.80), channel_id=1, replica_groups=mesh['ep'=8,'tp'=4] {'ep'}, dimensions={0} | all-to-all | bytes 4194304 | tf_op jit(solution)/shard_map/all_to_all | solution.py:93
  202.9 1.2 fusion.3
  204.1 0.9 copy-done.12
  205.1 1.3 fusion.11
  206.3 0.9 copy-done.13
  207.2 2.6 convolution_convert_fusion.1
  209.9 29.8 %reduce-scatter.5.cloned.1.call-done = bf16[8,32,1024]{2,1,0:T(8,128)(2,1)} async-done(((bf16[8,32,4096]{2,1,0:T(8,128)(2,1)}), bf16[8,32,1024]{2,1,0:T(8,128)(2,1)}) %reduce-scatter.5.cloned.1.call-update) | async-done | bytes 524304 | tf_op jit(solution)/shard_map/reduce_scatter | solution.py:100
  239.7 5.5 %all-to-all-start.2 = ((bf16[8,32,1024]{2,1,0:T(8,128)(2,1)}), bf16[8,32,1024]{2,1,0:T(8,128)(2,1)S(1)}, u32[]{:S(2)}, u32[]{:S(2)}) async-start(bf16[8,32,1024]{2,1,0:T(8,128)(2,1)} %reduce-scatter.5.cloned.1.call-done), calls=%async_computation.4 | async-start | bytes 1048576 | tf_op jit(solution)/shard_map/all_to_all | solution.py:103
  245.4 0.8 pad_maximum_fusion
  246.2 13.3 %all-to-all-done.2 = bf16[8,32,1024]{2,1,0:T(8,128)(2,1)S(1)} async-done(((bf16[8,32,1024]{2,1,0:T(8,128)(2,1)}), bf16[8,32,1024]{2,1,0:T(8,128)(2,1)S(1)}, u32[]{:S(2)}, u32[]{:S(2)}) %all-to-all-start.2) | async-done | bytes 524320 | tf_op jit(solution)/shard_map/all_to_all | solution.py:103
  259.7 1.6 add_convert_fusion
  (61 shorter events, 2.7 us)
Async XLA Ops:
  7.2 97.7 %copy-start = (bf16[4,256,256]{2,1,0:T(8,128)(2,1)S(1)}, bf16[4,256,256]{2,1,0:T(8,128)(2,1)}, u32[]{:S(2)}) copy-start(bf16[4,256,256]{2,1,0:T(8,128)(2,1)} %param.24) | copy-start | bytes 1572868
  7.2 96.7 %reduce-scatter.3.cloned.1.call-start = ((), (), s32[]{:S(2)}) async-start(), calls=%async_computation.5 | async-start | bytes 2359296 | tf_op jit(solution)/shard_map/reduce_scatter | solution.py:54
  32.1 4.3 %copy-start.3 = (bf16[64,3,1024]{2,0,1:T(8,128)(2,1)S(1)}, bf16[64,3,1024]{2,0,1:T(8,128)(2,1)}, u32[]{:S(2)}) copy-start(bf16[64,3,1024]{2,0,1:T(8,128)(2,1)} %param.19) | copy-start | bytes 1179652
  32.1 4.4 %copy-start.10 = (s32[64,2]{0,1:T(2,128)S(1)}, s32[64,2]{0,1:T(2,128)}, u32[]{:S(2)}) copy-start(s32[64,2]{0,1:T(2,128)} %param.32) | copy-start | bytes 1540
  32.1 4.9 %copy-start.8 = (f32[1024]{0:T(1024)S(1)}, f32[1024]{0:T(1024)}, u32[]{:S(2)}) copy-start(f32[1024]{0:T(1024)} %param.26) | copy-start | bytes 12292
  32.1 4.9 %copy-start.6 = (bf16[4,1024]{1,0:T(4,128)(2,1)S(1)}, bf16[4,1024]{1,0:T(4,128)(2,1)}, u32[]{:S(2)}) copy-start(bf16[4,1024]{1,0:T(4,128)(2,1)} %param.23) | copy-start | bytes 24580
  36.3 68.9 %copy-start.14 = (bf16[4,256,256]{2,1,0:T(8,128)(2,1)S(1)}, bf16[4,256,256]{2,1,0:T(8,128)(2,1)}, u32[]{:S(2)}) copy-start(bf16[4,256,256]{2,1,0:T(8,128)(2,1)} %param.25) | copy-start | bytes 1572868
  36.3 69.2 %copy-start.5 = (f32[64,1024]{1,0:T(8,128)S(1)}, f32[64,1024]{1,0:T(8,128)}, u32[]{:S(2)}) copy-start(f32[64,1024]{1,0:T(8,128)} %param.18) | copy-start | bytes 786436
  36.4 107.9 %all-reduce.2.cloned.1.call-start = ((), (), s32[]{:S(2)}) async-start(), calls=%async_computation.6 | async-start | bytes 1048576 | tf_op jit(solution)/shard_map/psum | solution.py:81
  103.8 1.9 copy-start.4
  105.7 5.9 %copy-start.2 = (f32[64,1024]{1,0:T(8,128)}, f32[64,1024]{1,0:T(8,128)S(1)}, u32[]{:S(2)}) copy-start(f32[64,1024]{1,0:T(8,128)S(1)} %multiply_add_fusion) | copy-start | bytes 786436
  105.7 6.2 %copy-start.7 = (bf16[4096]{0:T(1024)(128)(2,1)S(1)}, bf16[4096]{0:T(1024)(128)(2,1)}, u32[]{:S(2)}) copy-start(bf16[4096]{0:T(1024)(128)(2,1)} %param.28) | copy-start | bytes 24580
  105.8 38.5 %copy-start.1 = (bf16[64,4096]{1,0:T(8,128)(2,1)S(1)}, bf16[64,4096]{1,0:T(8,128)(2,1)}, u32[]{:S(2)}) copy-start(bf16[64,4096]{1,0:T(8,128)(2,1)} %param.17) | copy-start | bytes 1572868
  111.7 128.0 %reduce-scatter.5.cloned.1.call-start = ((), (), s32[]{:S(2)}) async-start(), calls=%async_computation.7 | async-start | bytes 2621440 | tf_op jit(solution)/shard_map/reduce_scatter | solution.py:100
  149.3 53.5 %copy-start.11 = (bf16[1,4096,512]{2,1,0:T(8,128)(2,1)S(1)}, bf16[1,4096,512]{2,1,0:T(8,128)(2,1)}, u32[]{:S(2)}) copy-start(bf16[1,4096,512]{2,1,0:T(8,128)(2,1)} %param.29) | copy-start | bytes 12582916
  202.9 2.2 copy-start.12
  205.1 2.2 copy-start.13
  207.2 38.1 %copy-start.9 = (f32[64,2]{0,1:T(2,128)S(1)}, f32[64,2]{0,1:T(2,128)}, u32[]{:S(2)}) copy-start(f32[64,2]{0,1:T(2,128)} %param.33) | copy-start | bytes 1540
  207.2 38.1 %slice-start = ((bf16[64,3,1024]{2,0,1:T(8,128)(2,1)}), bf16[64,2,1024]{2,0,1:T(8,128)(2,1)S(1)}, s32[]{:S(2)}) async-start(bf16[64,3,1024]{2,0,1:T(8,128)(2,1)} %param.19), calls=%async_computation.8 | async-start | bytes 524288 | tf_op jit(solution)/shard_map/slice | solution.py:63
  239.7 19.8 %all-to-all-start.2 = ((bf16[8,32,1024]{2,1,0:T(8,128)(2,1)}), bf16[8,32,1024]{2,1,0:T(8,128)(2,1)S(1)}, u32[]{:S(2)}, u32[]{:S(2)}) async-start(bf16[8,32,1024]{2,1,0:T(8,128)(2,1)} %reduce-scatter.5.cloned.1.call-done), calls=%async_computation.4 | async-start | bytes 1048576 | tf_op jit(solution)/shard_map/all_to_all | solution.py:103
Sparse Core Ops, SparseCore 0:
  36.5 67.3 reduce-scatter.2
  111.8 32.4 all-reduce.1
  210.0 29.6 reduce-scatter.4
where the time goes:
time: 269 us; the launch traced here: 268 us
  waiting for transfers between devices  142 us (53%)
  blocking collectives  74.4 us (28%)
  matrix products  16.6 us (6%)
  between operations  14.1 us (5%)
  other arithmetic  11.2 us (4%)
  starting transfers between devices  5.64 us (2%)
  local copies, waits for them, and re-layouts  3.75 us (1%)
    reduce_scatter x1, waiting for transfers between devices, shards(): lax.psum_scatter(jnp.dot(columns, joined, preferred_element_type=jnp.floa...  66.8 us
    all_to_all x1, blocking collectives, shards(): lax.all_to_all(send, 'ep', split_axis=0, concat_axis=0, tiled=True)  52.8 us
    psum x1, waiting for transfers between devices, shards(): lax.psum(partial_out.astype(jnp.bfloat16), 'tp').astype(jnp.float32)  32.4 us
    reduce_scatter x1, waiting for transfers between devices, shards(): lax.psum_scatter(partial_experts.astype(jnp.bfloat16), 'tp', scatter_dime...  29.8 us
    all_to_all x1, blocking collectives, shards(): lax.all_to_all(normed, 'ep', split_axis=1, concat_axis=0, tiled=True)  21.6 us
    all_to_all x1, waiting for transfers between devices, shards(): lax.all_to_all(reduced, 'ep', split_axis=0, concat_axis=0, tiled=True)  13.3 us
    dot_general x1, matrix products, shards(): partial_out = jnp.dot(gated, out_weight, preferred_element_type=jnp.float32)  5.88 us
    all_to_all x1, starting transfers between devices, shards(): lax.all_to_all(reduced, 'ep', split_axis=0, concat_axis=0, tiled=True)  5.51 us
  transfers between devices with their start and end apart: 4, of which 4 were waited for; matrix products, arithmetic and copies ran while one was open for 1% of the time, Pallas kernels for 0%

commit v1 on v0

v1 whole, which is shorter than its diff:
```python
import functools

import jax
import jax.numpy as jnp
from jax import lax
from jax.experimental import pallas as pl
from jax.experimental.pallas import tpu as pltpu
from jax.sharding import PartitionSpec as P

MESH = pl.DeviceIdType.MESH
F32 = jnp.float32
BF16 = jnp.bfloat16


def dot(a, b):
    return jnp.dot(a, b, preferred_element_type=F32)


def remote(src, dst, send, recv, where):
    return pltpu.make_async_remote_copy(
        src_ref=src, dst_ref=dst, send_sem=send, recv_sem=recv, device_id=where, device_id_type=MESH
    )


def kernel(
    n, p, cap,
    tokens, state_in, hist, mix_gain, moe_gain, conv_w, rate_param, routes, prob,
    rnn_h, gate_h, rate_h, input_h, out_h, eg_h, eu_h, ed_h,
    layer_out, state_out, moved_out,
    wr, wg, wrate, winput, wout, weg, weu, wed,
    normed, cols, part, rbuf, gated,
    op_p, op_o, op_r, hs, hr, mixed,
    sd, rows, xn, hid, e_p, e_o, e_r, es, er, outb, ret,
    wsem, sa, ra, sb, rb, sd1, rd1, sd2, rd2, sc1, rc1, sc2, rc2, sc3, rc3,
    se1, re1, se2, re2, se3, re3,
):
    e = lax.axis_index("ep")
    t = lax.axis_index("tp")
    core = lax.rem(t, 2)
    y = t // 2
    q = t + 1 - 2 * core
    ys = p // 2
    rows_g, width = tokens.shape
    depth = width // n
    chans = rnn_h.shape[1]
    share = width // p
    slots = n * cap

    loads = [
        pltpu.make_async_copy(a, b, wsem.at[i])
        for i, (a, b) in enumerate(
            [(rnn_h, wr), (gate_h, wg), (rate_h, wrate), (input_h, winput), (out_h, wout),
             (eg_h.at[0], weg), (eu_h.at[0], weu), (ed_h.at[0], wed)]
        )
    ]
    for load in loads:
        load.start()

    barrier = pltpu.get_barrier_semaphore()

    @pl.loop(1, n)
    def _(d):
        pl.semaphore_signal(barrier, inc=1, device_id={"ep": lax.rem(e + d, n)}, device_id_type=MESH)

    @pl.loop(1, p)
    def _(d):
        pl.semaphore_signal(barrier, inc=1, device_id={"tp": lax.rem(t + d, p)}, device_id_type=MESH)

    ssq = jnp.zeros((rows_g, 1), F32)
    for j in range(n):
        v = tokens[:, j * depth:(j + 1) * depth].astype(F32)
        ssq = ssq + jnp.sum(v * v, axis=1, keepdims=True)
    scale = lax.rsqrt(ssq / width + 1e-06)
    for j in range(n):
        cs = slice(j * depth, (j + 1) * depth)
        normed[j] = (tokens[:, cs].astype(F32) * scale * mix_gain[:, cs].astype(F32)).astype(BF16)

    pl.semaphore_wait(barrier, n + p - 2)

    def copy_a(d):
        peer = lax.rem(e + d, n)
        return remote(normed.at[peer], cols.at[e], sa.at[d], ra.at[d], {"ep": peer})

    @pl.loop(1, n)
    def _(d):
        copy_a(d).start()

    ids = routes[...]
    lane_e = lax.broadcasted_iota(jnp.int32, (rows_g, n), 1)
    named = [(ids[:, k:k + 1] == lane_e).astype(F32) for k in range(ids.shape[1])]
    member = functools.reduce(lambda a, b: a + b, named)
    earlier = (
        lax.broadcasted_iota(jnp.int32, (rows_g, rows_g), 1)
        < lax.broadcasted_iota(jnp.int32, (rows_g, rows_g), 0)
    ).astype(F32)
    before = dot(earlier.astype(BF16), member.astype(BF16))
    lane_s = lax.broadcasted_iota(jnp.int32, (rows_g, slots), 1).astype(F32)
    total_prob = jnp.sum(prob[...], axis=1, keepdims=True)
    dispatch = jnp.zeros((rows_g, slots), F32)
    comb = jnp.zeros((rows_g, slots), F32)
    for k in range(ids.shape[1]):
        slot = jnp.sum(before * named[k], axis=1, keepdims=True)
        target = ids[:, k:k + 1].astype(F32) * cap + slot
        hit = (lane_s == target).astype(F32)
        dispatch = dispatch + hit
        comb = comb + hit * (prob[:, k:k + 1] / total_prob)
    dispatch = dispatch.astype(BF16)
    comb_hi = comb.astype(BF16)
    comb_lo = (comb - comb_hi.astype(F32)).astype(BF16)

    loads[0].wait()
    loads[1].wait()
    rbuf[e, :, :chans] = dot(normed[e], wr[...]).astype(BF16)
    rbuf[e, :, chans:] = dot(normed[e], wg[...]).astype(BF16)

    def copy_b(d):
        peer = lax.rem(e - d + n, n)
        return remote(part.at[d], rbuf.at[e], sb.at[d], rb.at[d], {"ep": peer})

    @pl.loop(1, n)
    def _(d):
        src = lax.rem(e - d + n, n)
        copy_a(d).wait_recv()
        part[d, :, :chans] = dot(cols[src], wr[...]).astype(BF16)
        part[d, :, chans:] = dot(cols[src], wg[...]).astype(BF16)
        copy_b(d).start()

    @pl.loop(1, n)
    def _(d):
        copy_b(d).wait_recv()

    loads[2].wait()
    loads[3].wait()
    bw = rate_h.shape[1]
    for b in range(rate_h.shape[0]):
        cs = slice(b * bw, (b + 1) * bw)
        cy = slice(chans + b * bw, chans + (b + 1) * bw)
        proj_x = rbuf[0, :, cs].astype(F32)
        proj_y = rbuf[0, :, cy].astype(F32)
        for j in range(1, n):
            proj_x = proj_x + rbuf[j, :, cs].astype(F32)
            proj_y = proj_y + rbuf[j, :, cy].astype(F32)
        moved = proj_x.astype(BF16)
        moved_out[:, cs] = moved
        taps = conv_w[:, cs].astype(F32)
        conv = (hist[:, cs] + moved.astype(F32) * taps[3:4]).astype(BF16)
        rate = jax.nn.sigmoid(dot(conv, wrate[b]))
        in_gate = jax.nn.sigmoid(dot(conv, winput[b]))
        log_decay = -8.0 * rate * jnp.log1p(jnp.exp(-rate_param[:, cs]))
        th = jnp.tanh(log_decay)
        rest = -2.0 * th / (1.0 - th)
        state = jnp.exp(log_decay) * state_in[:, cs] + jnp.sqrt(rest) * in_gate * conv.astype(F32)
        state_out[:, cs] = state
        gated[:, cs] = (state * jax.nn.gelu(proj_y, approximate=True)).astype(BF16)

    def block(i):
        return pl.ds(pl.multiple_of(i * share, share), share)

    loads[4].wait()

    def copy_d1(yy):
        return remote(op_p.at[yy], op_r.at[yy], sd1.at[yy], rd1.at[yy], {"tp": q})

    def copy_d2(dy):
        ty = lax.rem(y + dy, ys)
        return remote(hs.at[ty], hr.at[y], sd2.at[dy], rd2.at[dy], {"tp": ty * 2 + core})

    for dy in range(ys):
        yy = lax.rem(y + dy + 1, ys)
        op_p[yy] = dot(gated[...], wout[:, block(yy * 2 + 1 - core)]).astype(BF16)
        copy_d1(yy).start()
    for dy in range(ys):
        yy = lax.rem(y + dy + 1, ys)
        op_o[yy] = dot(gated[...], wout[:, block(yy * 2 + core)])
    for dy in range(1, ys):
        ty = lax.rem(y + dy, ys)
        copy_d1(ty).wait_recv()
        hs[ty] = (op_o[ty] + op_r[ty].astype(F32)).astype(BF16)
        copy_d2(dy).start()
    copy_d1(y).wait_recv()
    total = tokens[:, block(t)].astype(F32) + op_o[y] + op_r[y].astype(F32)
    for dy in range(1, ys):
        copy_d2(dy).wait_recv()
        total = total + hr[lax.rem(y - dy + ys, ys)].astype(F32)
    mixed[...] = total

    sent = lax.dot_general(
        dispatch, mixed[...].astype(BF16), (((0,), (0,)), ((), ())), preferred_element_type=F32
    )
    sd[...] = sent.reshape(n, cap, share).astype(BF16)

    def copy_c1(d):
        peer = lax.rem(e + d, n)
        return remote(sd.at[peer], rows.at[t, e], sc1.at[d], rc1.at[d], {"ep": peer})

    def copy_c2(dy, d):
        src = lax.rem(e - d + n, n)
        to = lax.rem(y + dy, ys) * 2 + core
        return remote(rows.at[t, src], rows.at[t, src], sc2.at[dy, d], rc2.at[dy, d], {"tp": to})

    def copy_c3(dy, d):
        src = lax.rem(e - d + n, n)
        held = lax.rem(y - dy + ys, ys) * 2 + core
        return remote(rows.at[held, src], rows.at[held, src], sc3.at[dy, d], rc3.at[dy, d], {"tp": q})

    @pl.loop(1, n)
    def _(d):
        copy_c1(d).start()

    rows[t, e] = sd[e]

    def spread(d):
        for dy in range(1, ys):
            copy_c2(dy, d).start()
        copy_c3(0, d).start()

    spread(0)

    @pl.loop(1, n)
    def _(d):
        copy_c1(d).wait_recv()
        spread(d)

    @pl.loop(0, n)
    def _(d):
        for dy in range(1, ys):
            copy_c2(dy, d).wait_recv()
            copy_c3(dy, d).start()

    @pl.loop(0, n)
    def _(d):
        for dy in range(ys):
            copy_c3(dy, d).wait_recv()

    gs = min(n, max(1, 64 // cap))
    span = gs * cap

    @pl.loop(0, n // gs)
    def _(g):
        def piece(i):
            return rows[i, pl.ds(g * gs, gs)].astype(F32).reshape(span, share)

        acc = jnp.zeros((span, 1), F32)
        for i in range(p):
            v = piece(i)
            acc = acc + jnp.sum(v * v, axis=1, keepdims=True)
        sc = lax.rsqrt(acc / width + 1e-06)
        for i in range(p):
            cs = slice(i * share, (i + 1) * share)
            xn[pl.ds(pl.multiple_of(g * span, span), span), cs] = (
                piece(i) * sc * moe_gain[:, cs].astype(F32)
            ).astype(BF16)

    loads[5].wait()
    loads[6].wait()
    hidden = hid.shape[1]
    fc = min(256, hidden)

    @pl.loop(0, hidden // fc)
    def _(c):
        cs = pl.ds(pl.multiple_of(c * fc, fc), fc)
        gate_part = dot(xn[...], weg[:, cs])
        up_part = dot(xn[...], weu[:, cs])
        hid[:, cs] = (jax.nn.silu(gate_part) * up_part).astype(BF16)

    loads[7].wait()

    def copy_e1(yy):
        return remote(e_p.at[yy], e_r.at[yy], se1.at[yy], re1.at[yy], {"tp": q})

    def copy_e2(dy):
        ty = lax.rem(y + dy, ys)
        return remote(es.at[ty], er.at[y], se2.at[dy], re2.at[dy], {"tp": ty * 2 + core})

    def copy_e3(d):
        peer = lax.rem(e + d, n)
        return remote(outb.at[peer], ret.at[e], se3.at[d], re3.at[d], {"ep": peer})

    nc = min(256, share)

    def down(yy, parity, dst):
        @pl.loop(0, share // nc)
        def _(c):
            at = pl.ds(pl.multiple_of((yy * 2 + parity) * share + c * nc, nc), nc)
            dst[yy, :, pl.ds(pl.multiple_of(c * nc, nc), nc)] = dot(hid[...], wed[:, at]).astype(dst.dtype)

    for dy in range(ys):
        yy = lax.rem(y + dy + 1, ys)
        down(yy, 1 - core, e_p)
        copy_e1(yy).start()
    for dy in range(ys):
        down(lax.rem(y + dy + 1, ys), core, e_o)
    for dy in range(1, ys):
        ty = lax.rem(y + dy, ys)
        copy_e1(ty).wait_recv()
        es[ty] = (e_o[ty] + e_r[ty].astype(F32)).astype(BF16)
        copy_e2(dy).start()
    copy_e1(y).wait_recv()
    for dy in range(1, ys):
        copy_e2(dy).wait_recv()
    result = e_o[y] + e_r[y].astype(F32)
    for dy in range(1, ys):
        result = result + er[lax.rem(y - dy + ys, ys)].astype(F32)
    outb[...] = result.reshape(n, cap, share).astype(BF16)

    @pl.loop(1, n)
    def _(d):
        copy_e3(d).start()

    ret[e] = outb[e]

    @pl.loop(1, n)
    def _(d):
        copy_e3(d).wait_recv()

    back = ret[...].astype(F32).reshape(slots, share).astype(BF16)
    layer_out[...] = (mixed[...] + dot(comb_hi, back) + dot(comb_lo, back)).astype(BF16)

    @pl.loop(1, n)
    def _(d):
        copy_a(d).wait_send()
        copy_b(d).wait_send()
        copy_c1(d).wait_send()
        copy_e3(d).wait_send()

    @pl.loop(0, n)
    def _(d):
        for dy in range(1, ys):
            copy_c2(dy, d).wait_send()
        for dy in range(ys):
            copy_c3(dy, d).wait_send()

    for dy in range(ys):
        copy_d1(dy).wait_send()
        copy_e1(dy).wait_send()
    for dy in range(1, ys):
        copy_d2(dy).wait_send()
        copy_e2(dy).wait_send()


def shards(
    n, p,
    tokens, state_in, conv_in, mix_gain, rnn_weight, gate_weight, conv_weight, rate_weight,
    input_weight, rate_param, out_weight, moe_gain, expert_gate, expert_up, expert_down, routes, route_prob,
):
    g, width = tokens.shape
    depth, chans = rnn_weight.shape
    share = width // p
    cap = max(2, 2 * g * routes.shape[1] // n)
    slots = n * cap
    hidden = expert_gate.shape[2]
    ys = p // 2
    taps = conv_weight.astype(F32)
    history = conv_in.astype(F32)
    hist = history[:, 0] * taps[0] + history[:, 1] * taps[1] + history[:, 2] * taps[2]
    vm = pl.BlockSpec(memory_space=pltpu.VMEM)
    hb = pl.BlockSpec(memory_space=pl.ANY)
    dma = pltpu.SemaphoreType.DMA
    V = pltpu.VMEM
    scratch = [
        V((depth, chans), BF16), V((depth, chans), BF16),
        V(rate_weight.shape, BF16), V(input_weight.shape, BF16), V(out_weight.shape, BF16),
        V(expert_gate.shape[1:], BF16), V(expert_up.shape[1:], BF16), V(expert_down.shape[1:], BF16),
        V((n, g, depth), BF16), V((n, g, depth), BF16), V((n, g, 2 * chans), BF16), V((n, g, 2 * chans), BF16),
        V((g, chans), BF16),
        V((ys, g, share), BF16), V((ys, g, share), F32), V((ys, g, share), BF16),
        V((ys, g, share), BF16), V((ys, g, share), BF16), V((g, share), F32),
        V((n, cap, share), BF16), V((p, n, cap, share), BF16), V((slots, width), BF16), V((slots, hidden), BF16),
        V((ys, slots, share), BF16), V((ys, slots, share), F32), V((ys, slots, share), BF16),
        V((ys, slots, share), BF16), V((ys, slots, share), BF16),
        V((n, cap, share), BF16), V((n, cap, share), BF16),
        dma((8,)),
        dma((n,)), dma((n,)), dma((n,)), dma((n,)),
        dma((ys,)), dma((ys,)), dma((ys,)), dma((ys,)),
        dma((n,)), dma((n,)), dma((ys, n)), dma((ys, n)), dma((ys, n)), dma((ys, n)),
        dma((ys,)), dma((ys,)), dma((ys,)), dma((ys,)), dma((n,)), dma((n,)),
    ]
    layer_out, state_out, moved = pl.pallas_call(
        functools.partial(kernel, n, p, cap),
        out_shape=(
            jax.ShapeDtypeStruct((g, share), BF16),
            jax.ShapeDtypeStruct((g, chans), F32),
            jax.ShapeDtypeStruct((g, chans), BF16),
        ),
        in_specs=[vm] * 9 + [hb] * 8,
        out_specs=(vm, vm, vm),
        scratch_shapes=scratch,
        compiler_params=pltpu.CompilerParams(
            collective_id=0, has_side_effects=True, vmem_limit_bytes=60 * 1024 * 1024
        ),
    )(
        tokens, state_in, hist, mix_gain[None], moe_gain[None], conv_weight, rate_param[None], routes, route_prob,
        rnn_weight, gate_weight, rate_weight, input_weight, out_weight, expert_gate, expert_up, expert_down,
    )
    conv_out = jnp.concatenate([conv_in[:, 1:], moved[:, None, :]], axis=1)
    return (layer_out, state_out, conv_out)


def solution(mesh):
    in_specs = (
        P("ep", None),
        P("ep", "tp"),
        P("ep", None, "tp"),
        P(),
        P("ep", "tp"),
        P("ep", "tp"),
        P(None, "tp"),
        P("tp", None, None),
        P("tp", None, None),
        P("tp"),
        P("tp", None),
        P(),
        P("ep", None, "tp"),
        P("ep", None, "tp"),
        P("ep", "tp", None),
        P("ep", None),
        P("ep", None),
    )
    out_specs = (P("ep", "tp"), P("ep", "tp"), P("ep", None, "tp"))
    body = functools.partial(shards, mesh.shape["ep"], mesh.shape["tp"])
    return jax.shard_map(body, mesh=mesh, in_specs=in_specs, out_specs=out_specs, check_vma=False)
```

time: 269 us -> 156 us (0.58)
  waiting for transfers between devices: 142 us -> 0 us
  Pallas kernels: 0 us -> 141 us
  blocking collectives: 74.4 us -> 0 us
  matrix products: 16.6 us -> 0 us
  between operations: 14.1 us -> 0.66 us
  other arithmetic: 11.2 us -> 3.52 us
  local copies, waits for them, and re-layouts: 3.75 us -> 9.43 us
  starting transfers between devices: 5.64 us -> 0 us
    pallas_call x0 -> x1, Pallas kernels: none -> 141 us  [shards(): pl.pallas_call(functools.partial(kernel, n, p, cap), out_shape=(jax.Shape...]
    reduce_scatter x2 -> x0, waiting for transfers between devices: 96.6 us -> none  [the longest x1 66.8 us: shards(): lax.psum_scatter(jnp.dot(columns, joined, preferred_element_type=jnp.floa...]
    all_to_all x2 -> x0, blocking collectives: 74.4 us -> none  [the longest x1 52.8 us: shards(): lax.all_to_all(send, 'ep', split_axis=0, concat_axis=0, tiled=True)]
    psum x1 -> x0, waiting for transfers between devices: 32.4 us -> none  [shards(): lax.psum(partial_out.astype(jnp.bfloat16), 'tp').astype(jnp.float32)]
    dot_general x9 -> x0, matrix products: 16.6 us -> none  [the longest x1 5.88 us: shards(): partial_out = jnp.dot(gated, out_weight, preferred_element_type=jnp.float32)]
    all_to_all x1 -> x0, waiting for transfers between devices: 13.3 us -> none  [shards(): lax.all_to_all(reduced, 'ep', split_axis=0, concat_axis=0, tiled=True)]
    all_to_all x1 -> x0, starting transfers between devices: 5.51 us -> none  [shards(): lax.all_to_all(reduced, 'ep', split_axis=0, concat_axis=0, tiled=True)]
    convert_element_type x8 -> x1, other arithmetic: 6.13 us -> 1.07 us  [shards(): history = conv_in.astype(F32)]
  transfers between devices with their start and end apart: 4 -> 0, of which waited for: 4 -> 0; matrix products, arithmetic and copies ran while one was open for 1% -> 0% of each run, Pallas kernels for 0% -> 0%
where the time goes in v1:
time: 156 us; the launch traced here: 155 us
  Pallas kernels  141 us (90%)
  local copies, waits for them, and re-layouts  9.43 us (6%)
  other arithmetic  3.52 us (2%)
    pallas_call x1, Pallas kernels, shards(): pl.pallas_call(functools.partial(kernel, n, p, cap), out_shape=(jax.Shape...  141 us
    unnamed x4, local copies, waits for them, and re-layouts  6 us

profile of v1, /device:TPU:0, one launch (start us, length us, event | category | flops | bytes accessed | tf_op | source)
XLA Modules:
  0.0 154.7 jit_solution(3993051899056709726)
XLA Ops:
  0.6 1.1 convert_element_type.6
  1.7 0.8 fusion.5
  2.5 0.8 fusion.1.hist
  3.3 1.3 broadcast_in_dim.12.mix_gain
  4.6 1.3 broadcast_in_dim.13.moe_gain
  5.9 1.4 copy.20.routes
  7.3 1.4 copy.21.prob
  8.7 0.0 slice-start
  8.7 141.1 %shard_map.184 = (bf16[64,1024]{1,0:T(8,128)(2,1)}, f32[64,1024]{1,0:T(8,128)}, bf16[64,1024]{1,0:T(8,128)(2,1)}) custom-call(bf16[64,4096]{1,0:T(8,128)(2,1)} %tokens.1, f32[64,1024]{1,0:T(8,128)} %state_in.1, f32[64,1024]{1,0:T(8,128)} %fusion.1.hist, bf16[1,4096]{1,0:T(2,128)(2,1)} %broadcast_in_dim.12.mix_gain, ...), custom_call_target="tpu_custom_call" | custom-call | tf_op jit(solution)/shard_map/pallas_call | solution.py:378
  149.8 0.0 slice-done
  149.8 1.7 %pad_maximum_fusion = bf16[64,3,1024]{2,0,1:T(8,128)(2,1)} fusion(bf16[64,1,1024]{2,0,1:T(8,128)(2,1)} %bitcast.25, bf16[64,2,1024]{2,0,1:T(8,128)(2,1)S(1)} %slice-done), kind=kLoop, calls=%fused_computation | loop fusion | flops 196608 | bytes 786432 | tf_op jit(solution)/shard_map/concatenate | solution.py:395
  151.5 1.6 %copy.24 = bf16[64,1024]{1,0:T(8,128)(2,1)} copy(bf16[64,1024]{1,0:T(8,128)(2,1)} %get-tuple-element.15) | data formatting | bytes 262144
  153.0 1.7 %copy.25 = f32[64,1024]{1,0:T(8,128)} copy(f32[64,1024]{1,0:T(8,128)} %get-tuple-element.16) | data formatting | bytes 524288
Async XLA Ops:
  8.7 141.1 %slice-start = ((bf16[64,3,1024]{2,0,1:T(8,128)(2,1)}), bf16[64,2,1024]{2,0,1:T(8,128)(2,1)S(1)}, s32[]{:S(2)}) async-start(bf16[64,3,1024]{2,0,1:T(8,128)(2,1)} %param.19), calls=%async_computation | async-start | bytes 524288 | tf_op jit(solution)/shard_map/slice | solution.py:395

commit v2 on v1

v2 whole, which is shorter than its diff:
```python
import functools

import jax
import jax.numpy as jnp
from jax import lax
from jax.experimental import pallas as pl
from jax.experimental.pallas import tpu as pltpu
from jax.sharding import PartitionSpec as P

MESH = pl.DeviceIdType.MESH
F32 = jnp.float32
BF16 = jnp.bfloat16


def dot(a, b):
    return jnp.dot(a, b, preferred_element_type=F32)


def remote(src, dst, send, recv, where):
    return pltpu.make_async_remote_copy(
        src_ref=src, dst_ref=dst, send_sem=send, recv_sem=recv, device_id=where, device_id_type=MESH
    )


def kernel(
    n, p, nx, cap,
    tokens, state_in, conv_in, mix_gain_in, moe_gain_in, conv_w, rate_param, routes, prob,
    rnn_h, gate_h, rate_h, input_h, out_h, eg_h, eu_h, ed_h,
    layer_out, state_out, moved_out,
    wr, wg, wrate, winput, wout, weg, weu, wed,
    mix_gain, moe_gain, normed, cols, part, bx, zsend, rbuf, gated,
    op_p, op_o, op_r, hs, hr, mixed,
    sd, rows, xn, hid, e_p, e_o, e_r, es, er, outb, ret,
    wsem, sa, ra, sa2, ra2, sb, rb, sbz, rbz, sd1, rd1, sd2, rd2, sc1, rc1, sc2, rc2, sc3, rc3,
    se1, re1, se2, re2, se3, re3,
):
    e = lax.axis_index("ep")
    t = lax.axis_index("tp")
    core = lax.rem(t, 2)
    y = t // 2
    q = t + 1 - 2 * core
    ys = p // 2
    nz = n // nx
    z = e // nx
    x = lax.rem(e, nx)
    far_first = sorted(range(nz), key=lambda dz: -min(dz, nz - dz))

    def up(d):
        return lax.rem(z + d // nx, nz) * nx + lax.rem(x + d % nx, nx)

    def down_of(d):
        return lax.rem(z - d // nx + nz, nz) * nx + lax.rem(x - d % nx + nx, nx)

    rows_g, width = tokens.shape
    depth = width // n
    chans = rnn_h.shape[1]
    share = width // p
    slots = n * cap

    loads = [
        pltpu.make_async_copy(a, b, wsem.at[i])
        for i, (a, b) in enumerate(
            [(rnn_h, wr), (gate_h, wg), (rate_h, wrate), (input_h, winput), (out_h, wout),
             (eg_h.at[0], weg), (eu_h.at[0], weu), (ed_h.at[0], wed)]
        )
    ]
    for load in loads:
        load.start()

    barrier = pltpu.get_barrier_semaphore()

    @pl.loop(1, n)
    def _(d):
        pl.semaphore_signal(barrier, inc=1, device_id={"ep": lax.rem(e + d, n)}, device_id_type=MESH)

    @pl.loop(1, p)
    def _(d):
        pl.semaphore_signal(barrier, inc=1, device_id={"tp": lax.rem(t + d, p)}, device_id_type=MESH)

    for j in range(width // 128):
        cs = slice(j * 128, (j + 1) * 128)
        mix_gain[:, cs] = mix_gain_in[j:j + 1, :].astype(F32)
        moe_gain[:, cs] = moe_gain_in[j:j + 1, :].astype(F32)

    ssq = jnp.zeros((rows_g, 1), F32)
    for j in range(n):
        v = tokens[:, j * depth:(j + 1) * depth].astype(F32)
        ssq = ssq + jnp.sum(v * v, axis=1, keepdims=True)
    scale = lax.rsqrt(ssq / width + 1e-06)
    for j in range(n):
        cs = slice(j * depth, (j + 1) * depth)
        normed[j] = (tokens[:, cs].astype(F32) * scale * mix_gain[:, cs]).astype(BF16)

    pl.semaphore_wait(barrier, n + p - 2)

    half = pl.ds(pl.multiple_of(core * (rows_g // 2), rows_g // 2), rows_g // 2)

    def copy_a(d):
        peer = up(d)
        return remote(normed.at[peer, half], cols.at[e, half], sa.at[d], ra.at[d], {"ep": peer})

    def copy_a2(d):
        src = down_of(d)
        return remote(cols.at[src, half], cols.at[src, half], sa2.at[d], ra2.at[d], {"tp": q})

    for d in range(1, n):
        copy_a(d).start()
    cols[e] = normed[e]

    ids = routes[...]
    sub_e = lax.broadcasted_iota(jnp.int32, (n, rows_g), 0)
    named = [(ids[k:k + 1, :] == sub_e).astype(F32) for k in range(ids.shape[0])]
    member = functools.reduce(lambda a, b: a + b, named)
    earlier = (
        lax.broadcasted_iota(jnp.int32, (rows_g, rows_g), 0)
        < lax.broadcasted_iota(jnp.int32, (rows_g, rows_g), 1)
    ).astype(F32)
    before = dot(member.astype(BF16), earlier.astype(BF16))
    sub_s = lax.broadcasted_iota(jnp.int32, (slots, rows_g), 0).astype(F32)
    total_prob = jnp.sum(prob[...], axis=0, keepdims=True)
    dispatch = jnp.zeros((slots, rows_g), F32)
    comb = jnp.zeros((slots, rows_g), F32)
    for k in range(ids.shape[0]):
        slot = jnp.sum(before * named[k], axis=0, keepdims=True)
        target = ids[k:k + 1, :].astype(F32) * cap + slot
        hit = (sub_s == target).astype(F32)
        dispatch = dispatch + hit
        comb = comb + hit * (prob[k:k + 1, :] / total_prob)
    dispatch = dispatch.astype(BF16)
    comb_hi = comb.astype(BF16)
    comb_lo = (comb - comb_hi.astype(F32)).astype(BF16)

    loads[0].wait()
    loads[1].wait()

    def copy_b(dz, dx):
        zs = lax.rem(z - dz + nz, nz)
        peer = z * nx + lax.rem(x - dx + nx, nx)
        return remote(part.at[dz, dx], bx.at[dz, dx], sb.at[dz, dx], rb.at[dz, dx], {"ep": peer})

    def copy_bz(dz):
        peer = lax.rem(z - dz + nz, nz) * nx + x
        return remote(zsend.at[dz], rbuf.at[dz], sbz.at[dz], rbz.at[dz], {"ep": peer})

    def pass_on(dz):
        for lo in (0, chans):
            cs = slice(lo, lo + chans)
            if lo == 0:
                for dx in range(1, nx):
                    copy_b(dz, dx).wait_recv()
            acc = part[dz, 0, :, cs].astype(F32)
            for dx in range(1, nx):
                acc = acc + bx[dz, dx, :, cs].astype(F32)
            if dz:
                zsend[dz, :, cs] = acc.astype(BF16)
            else:
                rbuf[0, :, cs] = acc.astype(BF16)
        if dz:
            copy_bz(dz).start()

    for dz in range(nz):
        for dx in range(nx):
            d = dz * nx + dx
            if d:
                copy_a(d).wait_recv()
                copy_a2(d).start()
        for dx in list(range(1, nx)) + [0]:
            d = dz * nx + dx
            if d:
                copy_a2(d).wait_recv()
            src = down_of(d)
            part[dz, dx, :, :chans] = dot(cols[src], wr[...]).astype(BF16)
            part[dz, dx, :, chans:] = dot(cols[src], wg[...]).astype(BF16)
            if dx:
                copy_b(dz, dx).start()
        if dz >= 2:
            pass_on(dz - 1)
    pass_on(nz - 1)
    pass_on(0)
    for dz in range(1, nz):
        copy_bz(dz).wait_recv()

    loads[2].wait()
    loads[3].wait()
    bw = rate_h.shape[1]
    for b in range(rate_h.shape[0]):
        cs = slice(b * bw, (b + 1) * bw)
        cy = slice(chans + b * bw, chans + (b + 1) * bw)
        proj_x = rbuf[0, :, cs].astype(F32)
        proj_y = rbuf[0, :, cy].astype(F32)
        for j in range(1, nz):
            proj_x = proj_x + rbuf[j, :, cs].astype(F32)
            proj_y = proj_y + rbuf[j, :, cy].astype(F32)
        moved = proj_x.astype(BF16)
        moved_out[:, cs] = moved
        taps = conv_w[:, cs].astype(F32)
        hist = conv_in[0, :, cs].astype(F32) * taps[0:1]
        for i in range(1, 3):
            hist = hist + conv_in[i, :, cs].astype(F32) * taps[i:i + 1]
        conv = (hist + moved.astype(F32) * taps[3:4]).astype(BF16)
        rate = jax.nn.sigmoid(dot(conv, wrate[b]))
        in_gate = jax.nn.sigmoid(dot(conv, winput[b]))
        log_decay = -8.0 * rate * jnp.log1p(jnp.exp(-rate_param[:, cs]))
        th = jnp.tanh(log_decay)
        rest = -2.0 * th / (1.0 - th)
        state = jnp.exp(log_decay) * state_in[:, cs] + jnp.sqrt(rest) * in_gate * conv.astype(F32)
        state_out[:, cs] = state
        gated[:, cs] = (state * jax.nn.gelu(proj_y, approximate=True)).astype(BF16)

    def block(i):
        return pl.ds(pl.multiple_of(i * share, share), share)

    loads[4].wait()

    def copy_d1(yy):
        return remote(op_p.at[yy], op_r.at[yy], sd1.at[yy], rd1.at[yy], {"tp": q})

    def copy_d2(dy):
        ty = lax.rem(y + dy, ys)
        return remote(hs.at[ty], hr.at[y], sd2.at[dy], rd2.at[dy], {"tp": ty * 2 + core})

    for dy in range(ys):
        yy = lax.rem(y + dy + 1, ys)
        op_p[yy] = dot(gated[...], wout[:, block(yy * 2 + 1 - core)]).astype(BF16)
        copy_d1(yy).start()
    for dy in range(ys):
        yy = lax.rem(y + dy + 1, ys)
        op_o[yy] = dot(gated[...], wout[:, block(yy * 2 + core)])
    for dy in range(1, ys):
        ty = lax.rem(y + dy, ys)
        copy_d1(ty).wait_recv()
        hs[ty] = (op_o[ty] + op_r[ty].astype(F32)).astype(BF16)
        copy_d2(dy).start()
    copy_d1(y).wait_recv()
    total = tokens[:, block(t)].astype(F32) + op_o[y] + op_r[y].astype(F32)
    for dy in range(1, ys):
        copy_d2(dy).wait_recv()
        total = total + hr[lax.rem(y - dy + ys, ys)].astype(F32)
    mixed[...] = total

    sent = dot(dispatch, mixed[...].astype(BF16))
    sd[...] = sent.reshape(n, cap, share).astype(BF16)

    def copy_c1(d):
        peer = up(d)
        return remote(sd.at[peer], rows.at[t, e], sc1.at[d], rc1.at[d], {"ep": peer})

    def copy_c2(dy, d):
        src = down_of(d)
        to = lax.rem(y + dy, ys) * 2 + core
        return remote(rows.at[t, src], rows.at[t, src], sc2.at[dy, d], rc2.at[dy, d], {"tp": to})

    def copy_c3(dy, d):
        src = down_of(d)
        held = lax.rem(y - dy + ys, ys) * 2 + core
        return remote(rows.at[held, src], rows.at[held, src], sc3.at[dy, d], rc3.at[dy, d], {"tp": q})

    order = [dz * nx + dx for dz in far_first for dx in range(nx) if dz + dx]
    for d in order:
        copy_c1(d).start()

    rows[t, e] = sd[e]

    def spread(d):
        for dy in range(1, ys):
            copy_c2(dy, d).start()
        copy_c3(0, d).start()

    def relay(d):
        for dy in range(1, ys):
            copy_c2(dy, d).wait_recv()
            copy_c3(dy, d).start()

    near = order[::-1]
    spread(0)
    for i, d in enumerate(near):
        copy_c1(d).wait_recv()
        spread(d)
        if i >= 1:
            relay(([0] + near)[i - 1])
    for d in ([0] + near)[len(near) - 1:]:
        relay(d)
    for d in range(n):
        for dy in range(ys):
            copy_c3(dy, d).wait_recv()

    gs = min(n, max(1, 64 // cap))
    span = gs * cap

    @pl.loop(0, n // gs)
    def _(g):
        def piece(i):
            return rows[i, pl.ds(g * gs, gs)].astype(F32).reshape(span, share)

        acc = jnp.zeros((span, 1), F32)
        for i in range(p):
            v = piece(i)
            acc = acc + jnp.sum(v * v, axis=1, keepdims=True)
        sc = lax.rsqrt(acc / width + 1e-06)
        for i in range(p):
            cs = slice(i * share, (i + 1) * share)
            xn[pl.ds(pl.multiple_of(g * span, span), span), cs] = (
                piece(i) * sc * moe_gain[:, cs]
            ).astype(BF16)

    loads[5].wait()
    loads[6].wait()
    hidden = hid.shape[1]
    fc = min(256, hidden)

    @pl.loop(0, hidden // fc)
    def _(c):
        cs = pl.ds(pl.multiple_of(c * fc, fc), fc)
        gate_part = dot(xn[...], weg[:, cs])
        up_part = dot(xn[...], weu[:, cs])
        hid[:, cs] = (jax.nn.silu(gate_part) * up_part).astype(BF16)

    loads[7].wait()

    def copy_e1(yy):
        return remote(e_p.at[yy], e_r.at[yy], se1.at[yy], re1.at[yy], {"tp": q})

    def copy_e2(dy, dz):
        ty = lax.rem(y + dy, ys)
        zc = lax.rem(z + dz, nz)
        return remote(
            es.at[ty, zc], er.at[y, zc], se2.at[dy, dz], re2.at[dy, dz], {"tp": ty * 2 + core}
        )

    def copy_e3(d):
        peer = up(d)
        return remote(outb.at[peer], ret.at[e], se3.at[d], re3.at[d], {"ep": peer})

    nc = min(256, share)
    chunk = nx * cap

    def down(yy, parity, dst):
        @pl.loop(0, share // nc)
        def _(c):
            at = pl.ds(pl.multiple_of((yy * 2 + parity) * share + c * nc, nc), nc)
            value = dot(hid[...], wed[:, at]).reshape(nz, chunk, nc)
            dst[yy, :, :, pl.ds(pl.multiple_of(c * nc, nc), nc)] = value.astype(dst.dtype)

    for dy in list(range(1, ys)) + [0]:
        ty = lax.rem(y + dy, ys)
        down(ty, 1 - core, e_p)
        copy_e1(ty).start()
        down(ty, core, e_o)
        copy_e1(ty).wait_recv()
        if dy:
            for dz in far_first:
                zc = lax.rem(z + dz, nz)
                es[ty, zc] = (e_o[ty, zc] + e_r[ty, zc].astype(F32)).astype(BF16)
                copy_e2(dy, dz).start()
    for dz in far_first:
        zc = lax.rem(z + dz, nz)
        result = e_o[y, zc] + e_r[y, zc].astype(F32)
        for dy in range(1, ys):
            copy_e2(dy, dz).wait_recv()
            result = result + er[lax.rem(y - dy + ys, ys), zc].astype(F32)
        outb[pl.ds(zc * nx, nx)] = result.reshape(nx, cap, share).astype(BF16)
        for dx in range(nx):
            if dz + dx:
                copy_e3(dz * nx + dx).start()

    ret[e] = outb[e]
    for d in order:
        copy_e3(d).wait_recv()

    back = ret[...].astype(F32).reshape(slots, share).astype(BF16)

    def combine(weights):
        return lax.dot_general(weights, back, (((0,), (0,)), ((), ())), preferred_element_type=F32)

    layer_out[...] = (mixed[...] + combine(comb_hi) + combine(comb_lo)).astype(BF16)

    @pl.loop(1, n)
    def _(d):
        copy_a(d).wait_send()
        copy_a2(d).wait_send()
        copy_c1(d).wait_send()
        copy_e3(d).wait_send()

    @pl.loop(0, n)
    def _(d):
        for dy in range(1, ys):
            copy_c2(dy, d).wait_send()
        for dy in range(ys):
            copy_c3(dy, d).wait_send()

    for dy in range(ys):
        copy_d1(dy).wait_send()
        copy_e1(dy).wait_send()
    for dy in range(1, ys):
        copy_d2(dy).wait_send()
        for dz in range(nz):
            copy_e2(dy, dz).wait_send()
    for dz in range(nz):
        for dx in range(1, nx):
            copy_b(dz, dx).wait_send()
        if dz:
            copy_bz(dz).wait_send()


def finish(layer_in, state_in, moved, conv_in, layer_out, state_out, conv_out):
    layer_out[...] = layer_in[...]
    state_out[...] = state_in[...]
    kept = conv_in.shape[0] - 1
    for i in range(kept):
        conv_out[i] = conv_in[i + 1]
    conv_out[kept] = moved[...]


def shards(
    n, p,
    tokens, state_in, conv_in, mix_gain, rnn_weight, gate_weight, conv_weight, rate_weight,
    input_weight, rate_param, out_weight, moe_gain, expert_gate, expert_up, expert_down, routes, route_prob,
):
    g, width = tokens.shape
    depth, chans = rnn_weight.shape
    share = width // p
    cap = max(2, 2 * g * routes.shape[1] // n)
    slots = n * cap
    hidden = expert_gate.shape[2]
    ys = p // 2
    nx = 1 << ((n.bit_length() - 1) // 2)
    nx = nx if n % nx == 0 else 1
    nz = n // nx
    conv_t = jnp.transpose(conv_in, (1, 0, 2))
    vm = pl.BlockSpec(memory_space=pltpu.VMEM)
    hb = pl.BlockSpec(memory_space=pl.ANY)
    dma = pltpu.SemaphoreType.DMA
    V = pltpu.VMEM
    scratch = [
        V((depth, chans), BF16), V((depth, chans), BF16),
        V(rate_weight.shape, BF16), V(input_weight.shape, BF16), V(out_weight.shape, BF16),
        V(expert_gate.shape[1:], BF16), V(expert_up.shape[1:], BF16), V(expert_down.shape[1:], BF16),
        V((1, width), F32), V((1, width), F32),
        V((n, g, depth), BF16), V((n, g, depth), BF16),
        V((nz, nx, g, 2 * chans), BF16), V((nz, nx, g, 2 * chans), BF16),
        V((nz, g, 2 * chans), BF16), V((nz, g, 2 * chans), BF16),
        V((g, chans), BF16),
        V((ys, g, share), BF16), V((ys, g, share), F32), V((ys, g, share), BF16),
        V((ys, g, share), BF16), V((ys, g, share), BF16), V((g, share), F32),
        V((n, cap, share), BF16), V((p, n, cap, share), BF16), V((slots, width), BF16), V((slots, hidden), BF16),
        V((ys, nz, nx * cap, share), BF16), V((ys, nz, nx * cap, share), F32), V((ys, nz, nx * cap, share), BF16),
        V((ys, nz, nx * cap, share), BF16), V((ys, nz, nx * cap, share), BF16),
        V((n, cap, share), BF16), V((n, cap, share), BF16),
        dma((8,)),
        dma((n,)), dma((n,)), dma((n,)), dma((n,)), dma((nz, nx)), dma((nz, nx)), dma((nz,)), dma((nz,)),
        dma((ys,)), dma((ys,)), dma((ys,)), dma((ys,)),
        dma((n,)), dma((n,)), dma((ys, n)), dma((ys, n)), dma((ys, n)), dma((ys, n)),
        dma((ys,)), dma((ys,)), dma((ys, nz)), dma((ys, nz)), dma((n,)), dma((n,)),
    ]
    layer, state, moved = pl.pallas_call(
        functools.partial(kernel, n, p, nx, cap),
        out_shape=(
            jax.ShapeDtypeStruct((g, share), BF16),
            jax.ShapeDtypeStruct((g, chans), F32),
            jax.ShapeDtypeStruct((g, chans), BF16),
        ),
        in_specs=[vm] * 9 + [hb] * 8,
        out_specs=(vm, vm, vm),
        scratch_shapes=scratch,
        compiler_params=pltpu.CompilerParams(
            collective_id=0, has_side_effects=True, vmem_limit_bytes=60 * 1024 * 1024
        ),
    )(
        tokens, state_in, conv_t, mix_gain.reshape(-1, 128), moe_gain.reshape(-1, 128),
        conv_weight, rate_param[None], routes.T, route_prob.T,
        rnn_weight, gate_weight, rate_weight, input_weight, out_weight, expert_gate, expert_up, expert_down,
    )
    layer_out, state_out, conv_out = pl.pallas_call(
        finish,
        out_shape=(
            jax.ShapeDtypeStruct(layer.shape, layer.dtype),
            jax.ShapeDtypeStruct(state.shape, state.dtype),
            jax.ShapeDtypeStruct(conv_t.shape, conv_t.dtype),
        ),
        in_specs=[vm] * 4,
        out_specs=(vm, vm, vm),
    )(layer, state, moved, conv_t)
    return (layer_out, state_out, jnp.transpose(conv_out, (1, 0, 2)))


def solution(mesh):
    in_specs = (
        P("ep", None),
        P("ep", "tp"),
        P("ep", None, "tp"),
        P(),
        P("ep", "tp"),
        P("ep", "tp"),
        P(None, "tp"),
        P("tp", None, None),
        P("tp", None, None),
        P("tp"),
        P("tp", None),
        P(),
        P("ep", None, "tp"),
        P("ep", None, "tp"),
        P("ep", "tp", None),
        P("ep", None),
        P("ep", None),
    )
    out_specs = (P("ep", "tp"), P("ep", "tp"), P("ep", None, "tp"))
    body = functools.partial(shards, mesh.shape["ep"], mesh.shape["tp"])
    return jax.shard_map(body, mesh=mesh, in_specs=in_specs, out_specs=out_specs, check_vma=False)
```

time: 156 us -> 109 us (0.70)
  Pallas kernels: 141 us -> 108 us
  local copies, waits for them, and re-layouts: 9.43 us -> 0 us
  other arithmetic: 3.52 us -> 0 us
    pallas_call x1 -> x2, Pallas kernels: 141 us -> 108 us  [the longest x1 106 us: shards(): pl.pallas_call(functools.partial(kernel, n, p, nx, cap), out_shape=(jax.S...]
    unnamed x4 -> x0, local copies, waits for them, and re-layouts: 6 us -> none
    broadcast_in_dim x2 -> x0, local copies, waits for them, and re-layouts: 2.61 us -> none  [the longest x1 1.31 us: shards(): moe_gain[None]]
    concatenate x1 -> x0, other arithmetic: 1.69 us -> none  [shards(): conv_out = jnp.concatenate([conv_in[:, 1:], moved[:, None, :]], axis=1)]
where the time goes in v2:
time: 109 us
  Pallas kernels  108 us (99%)
    pallas_call x1, Pallas kernels, shards(): pl.pallas_call(functools.partial(kernel, n, p, nx, cap), out_shape=(jax.S...  106 us

profile of v2, /device:TPU:0, one launch (start us, length us, event | category | flops | bytes accessed | tf_op | source)
XLA Modules:
  0.0 108.5 jit_solution(7670486851475880389)
XLA Ops:
  0.6 105.8 %shard_map.184 = (bf16[64,1024]{1,0:T(8,128)(2,1)}, f32[64,1024]{1,0:T(8,128)}, bf16[64,1024]{1,0:T(8,128)(2,1)}) custom-call(bf16[64,4096]{1,0:T(8,128)(2,1)} %tokens.1, f32[64,1024]{1,0:T(8,128)} %state_in.1, bf16[3,64,1024]{2,1,0:T(8,128)(2,1)} %bitcast.7, bf16[32,128]{1,0:T(8,128)(2,1)} %bitcast.9, bf16[32,128]{1,0:T(8,128)(2,1)} %bitcast.10, ...), custom_call_target="tpu_custom_call" | custom-call | tf_op jit(solution)/shard_map/pallas_call | solution.py:455
  106.4 2.1 %shard_map.185 = (bf16[64,1024]{1,0:T(8,128)(2,1)}, f32[64,1024]{1,0:T(8,128)}, bf16[3,64,1024]{2,1,0:T(8,128)(2,1)}) custom-call(bf16[64,1024]{1,0:T(8,128)(2,1)} %get-tuple-element.9.layer_in, f32[64,1024]{1,0:T(8,128)} %get-tuple-element.10.state_in, bf16[64,1024]{1,0:T(8,128)(2,1)} %get-tuple-element.11.moved, bf16[3,64,1024]{2,1,0:T(8,128)(2,1)} %bitcast.8), custom_call_target="tpu_custom_call" | custom-call | tf_op jit(solution)/shard_map/pallas_call | solution.py:473

commit v3 on v2

--- a/solution.py
+++ b/solution.py
@@ -64,7 +64,7 @@
              (eg_h.at[0], weg), (eu_h.at[0], weu), (ed_h.at[0], wed)]
         )
     ]
-    for load in loads:
+    for load in loads[:4]:
         load.start()
 
     barrier = pltpu.get_barrier_semaphore()
@@ -103,8 +103,11 @@
         src = down_of(d)
         return remote(cols.at[src, half], cols.at[src, half], sa2.at[d], ra2.at[d], {"tp": q})
 
-    for d in range(1, n):
-        copy_a(d).start()
+    away_first = list(range(1, nz)) + [0]
+    for dz in away_first:
+        for dx in range(nx):
+            if dz + dx:
+                copy_a(dz * nx + dx).start()
     cols[e] = normed[e]
 
     ids = routes[...]
@@ -132,6 +135,8 @@
 
     loads[0].wait()
     loads[1].wait()
+    for load in loads[4:]:
+        load.start()
 
     def copy_b(dz, dx):
         zs = lax.rem(z - dz + nz, nz)
@@ -158,7 +163,7 @@
         if dz:
             copy_bz(dz).start()
 
-    for dz in range(nz):
+    for k, dz in enumerate(away_first):
         for dx in range(nx):
             d = dz * nx + dx
             if d:
@@ -173,9 +178,8 @@
             part[dz, dx, :, chans:] = dot(cols[src], wg[...]).astype(BF16)
             if dx:
                 copy_b(dz, dx).start()
-        if dz >= 2:
-            pass_on(dz - 1)
-    pass_on(nz - 1)
+        if k:
+            pass_on(away_first[k - 1])
     pass_on(0)
     for dz in range(1, nz):
         copy_bz(dz).wait_recv()

time: 109 us -> 105 us (0.963)
  Pallas kernels: 108 us -> 104 us
    pallas_call x1, Pallas kernels: 106 us -> 102 us  [shards(): pl.pallas_call(functools.partial(kernel, n, p, nx, cap), out_shape=(jax.S...]
where the time goes in v3:
time: 105 us; the launch traced here: 104 us
  Pallas kernels  104 us (99%)
    pallas_call x1, Pallas kernels, shards(): pl.pallas_call(functools.partial(kernel, n, p, nx, cap), out_shape=(jax.S...  102 us

profile of v3, /device:TPU:0, one launch (start us, length us, event | category | flops | bytes accessed | tf_op | source)
XLA Modules:
  0.0 104.5 jit_solution(13617468371669196236)
XLA Ops:
  0.6 101.8 %shard_map.184 = (bf16[64,1024]{1,0:T(8,128)(2,1)}, f32[64,1024]{1,0:T(8,128)}, bf16[64,1024]{1,0:T(8,128)(2,1)}) custom-call(bf16[64,4096]{1,0:T(8,128)(2,1)} %tokens.1, f32[64,1024]{1,0:T(8,128)} %state_in.1, bf16[3,64,1024]{2,1,0:T(8,128)(2,1)} %bitcast.7, bf16[32,128]{1,0:T(8,128)(2,1)} %bitcast.9, bf16[32,128]{1,0:T(8,128)(2,1)} %bitcast.10, ...), custom_call_target="tpu_custom_call" | custom-call | tf_op jit(solution)/shard_map/pallas_call | solution.py:459
  102.4 2.1 %shard_map.185 = (bf16[64,1024]{1,0:T(8,128)(2,1)}, f32[64,1024]{1,0:T(8,128)}, bf16[3,64,1024]{2,1,0:T(8,128)(2,1)}) custom-call(bf16[64,1024]{1,0:T(8,128)(2,1)} %get-tuple-element.9.layer_in, f32[64,1024]{1,0:T(8,128)} %get-tuple-element.10.state_in, bf16[64,1024]{1,0:T(8,128)(2,1)} %get-tuple-element.11.moved, bf16[3,64,1024]{2,1,0:T(8,128)(2,1)} %bitcast.8), custom_call_target="tpu_custom_call" | custom-call | tf_op jit(solution)/shard_map/pallas_call | solution.py:477
